TPU v7x, 256 devices: a whole 4x4x8 slice. The times are simulated.
256 devices in a mesh: ep: 16 (over y, x), tp: 16 (over z, core).
Axes of the slice: x: 4, y: 4, z: 8, core: 2. Of those that a mesh axis runs over, the one named last changes fastest.
Arguments:
- stream: bfloat16 [256, 2048], P('ep'), may hold values from -6 to 6
- norm_gain_attn: float32 [2048], replicated, may hold values from 0.1 to 1.9
- w_query: bfloat16 [2048, 2048], P('ep', 'tp'), may hold values from -0.125 to 0.125
- w_key: bfloat16 [2048, 2048], P('ep', 'tp'), may hold values from -0.125 to 0.125
- w_value: bfloat16 [2048, 2048], P('ep', 'tp'), may hold values from -0.125 to 0.125
- w_forget: bfloat16 [2048, 16], replicated, may hold values from -0.125 to 0.125
- forget_bias: float32 [16], replicated, may hold values from -2 to 2
- key_cache: bfloat16 [256, 1024, 2048], P('ep', None, 'tp'), may hold values from -1500 to 1500
- value_cache: bfloat16 [256, 1024, 2048], P('ep', None, 'tp'), may hold values from -6 to 6
- gate_cache: float32 [256, 16, 1024], P('ep', 'tp'), may hold values from -1024 to 0, as said below
- lengths: int32 [256], P('ep'), may hold values from 128 to 1024
- w_output: bfloat16 [2048, 2048], P('tp'), may hold values from -0.125 to 0.125
- norm_gain_ffn: float32 [2048], replicated, may hold values from 0.1 to 1.9
- routes: int32 [256, 2], replicated, may hold values from 0 to 15, all different within a row; in each aligned block of 16 rows (0 to 15, 16 to 31, ...) at most 4 rows name the same one
- route_weights: float32 [256, 2], replicated, may hold values from 0.2 to 1
- w_expert_gate: bfloat16 [16, 2048, 5632], P('ep', None, 'tp'), may hold values from -0.125 to 0.125
- w_expert_up: bfloat16 [16, 2048, 5632], P('ep', None, 'tp'), may hold values from -0.125 to 0.125
- expert_down_weight: bfloat16 [16, 5632, 2048], P('ep', 'tp'), may hold values from -0.078125 to 0.078125
Outputs:
- result: bfloat16 [256, 2048], P('ep', 'tp')
Inputs may be any that keep to these rules, and one draw needn't show every extreme that they name: `gate_cache`: never rises along positions. `routes`: in the rows of one index of ep no expert is named by more than 4 rows, and in some such block one is named by exactly 4.
All inputs are finite; a program needn't handle non-finite values.
Results may differ from a plain program's by a relative error of at most 0.014.
Values may be sent and summed in bfloat16 or wider, within the bound.
A program may use at most 64 MiB of HBM per device.

v0:
```python
import jax
import jax.numpy as jnp
from jax import lax
from jax.sharding import PartitionSpec as P


def split_up(shard, dim, peers):
    before, after = (shard.shape[:dim], shard.shape[dim + 1 :])
    return jnp.moveaxis(shard.reshape(*before, peers, -1, *after), dim, 0)


def sent_and_summed(shard, axis, dim):
    peers = lax.axis_size(axis)
    blocks = lax.all_to_all(split_up(shard, dim, peers), axis, 0, 0, tiled=True)
    return jnp.sum(blocks.astype(jnp.float32), axis=0)


def sum_at_owner(shard, axis, dim):
    blocks = split_up(shard, dim, lax.axis_size(axis))
    arrived = lax.all_to_all(blocks, axis, split_axis=0, concat_axis=0, tiled=True)
    return arrived.sum(axis=0)


def from_everyone(shard, axis):
    copies = jnp.broadcast_to(shard, (lax.axis_size(axis), *shard.shape))
    return lax.all_to_all(copies, axis, split_axis=0, concat_axis=0, tiled=True)


def taken_together(shard, axis):
    return from_everyone(shard, axis).astype(jnp.float32).sum(axis=0)


def rms_norm(values, gain):
    floats = values.astype(jnp.float32)
    scaled = floats * lax.rsqrt(jnp.mean(floats * floats, axis=-1, keepdims=True) + 1e-06)
    return (scaled * gain).astype(jnp.bfloat16)


def expert_rows(inputs, w_expert_gate, w_expert_up, expert_down_weight):
    hidden = (
        jax.nn.silu(jnp.dot(inputs, w_expert_gate[0], preferred_element_type=jnp.float32))
        * jnp.dot(inputs, w_expert_up[0], preferred_element_type=jnp.float32)
    ).astype(jnp.bfloat16)
    partial_out = jnp.dot(hidden, expert_down_weight[0], preferred_element_type=jnp.float32)
    return sent_and_summed(partial_out.astype(jnp.bfloat16), "tp", 1).astype(jnp.bfloat16)


def shards(
    stream,
    norm_gain_attn,
    w_query,
    w_key,
    w_value,
    w_forget,
    forget_bias,
    key_cache,
    value_cache,
    gate_cache,
    lengths,
    w_output,
    norm_gain_ffn,
    routes,
    route_weights,
    w_expert_gate,
    w_expert_up,
    expert_down_weight,
):
    seq_count = stream.shape[0]
    model_width = stream.shape[1]
    groups = lax.axis_size("ep")
    group_index = lax.axis_index("ep")
    width_index = lax.axis_index("tp")
    heads_here = gate_cache.shape[1]
    cache_len = key_cache.shape[1]
    head_dim = key_cache.shape[2] // heads_here
    width_per_device = heads_here * head_dim
    normed = rms_norm(stream, norm_gain_attn)
    spread = lax.all_to_all(normed, "ep", split_axis=1, concat_axis=0, tiled=True)
    stacked = jnp.concatenate([w_query, w_key, w_value], axis=1)
    block = spread
    projected = sum_at_owner(jnp.dot(block, stacked, preferred_element_type=jnp.float32), "ep", 0)
    query = (
        projected[:, :width_per_device]
        .astype(jnp.bfloat16)
        .reshape(seq_count, heads_here, head_dim)
    )
    key_new = (
        projected[:, width_per_device : 2 * width_per_device]
        .astype(jnp.bfloat16)
        .reshape(seq_count, heads_here, head_dim)
    )
    value_new = (
        projected[:, 2 * width_per_device :]
        .astype(jnp.bfloat16)
        .reshape(seq_count, heads_here, head_dim)
    )
    forget_all = jax.nn.log_sigmoid(
        jnp.dot(normed, w_forget, preferred_element_type=jnp.float32) + forget_bias
    )
    forget_new = lax.dynamic_slice_in_dim(forget_all, width_index * heads_here, heads_here, 1)
    scale = head_dim ** (-0.5)
    keys = key_cache.reshape(seq_count, cache_len, heads_here, head_dim)
    values = value_cache.reshape(seq_count, cache_len, heads_here, head_dim)
    sequence_indices = jnp.arange(cache_len, dtype=jnp.int32)
    is_live = sequence_indices[None, None, :] < lengths[:, None, None]
    last_gate = jnp.sum(
        jnp.where(sequence_indices[None, None, :] == lengths[:, None, None] - 1, gate_cache, 0.0),
        axis=-1,
    )
    scores = jnp.einsum("shd,sphd->shp", query, keys, preferred_element_type=jnp.float32) * scale
    scores = scores + forget_new[..., None] + last_gate[..., None] - gate_cache
    own_score = (
        jnp.einsum("shd,shd->sh", query, key_new, preferred_element_type=jnp.float32) * scale
    )
    hidden_from_view = jnp.where(is_live, scores, -1e30)
    largest = jnp.maximum(jnp.max(hidden_from_view, axis=-1), own_score)
    past = jnp.exp(hidden_from_view - largest[..., None])
    own_term = jnp.exp(own_score - largest)
    total = jnp.sum(past, axis=-1) + own_term
    past_weights = (past / total[..., None]).astype(jnp.bfloat16)
    own_weights = lax.optimization_barrier((own_term / total).astype(jnp.bfloat16))
    attended = jnp.einsum("shp,sphd->shd", past_weights, values, preferred_element_type=jnp.float32)
    attended = attended + own_weights.astype(jnp.float32)[..., None] * value_new.astype(jnp.float32)
    attended = attended.reshape(seq_count, width_per_device).astype(jnp.bfloat16)
    head_total = taken_together(
        jnp.dot(attended, w_output, preferred_element_type=jnp.float32).astype(jnp.bfloat16), "tp"
    ).astype(jnp.float32)
    mixed = (stream.astype(jnp.float32) + head_total).astype(jnp.bfloat16)
    normed_ffn = rms_norm(mixed, norm_gain_ffn)
    top_count = routes.shape[1]
    capacity = 2 * seq_count * top_count // groups
    slice_width = model_width // lax.axis_size("tp")
    own_stream = lax.dynamic_slice_in_dim(mixed, width_index * slice_width, slice_width, 1)
    my_routes = lax.dynamic_slice_in_dim(routes, group_index * seq_count, seq_count, 0).reshape(-1)
    my_weights = lax.dynamic_slice_in_dim(route_weights, group_index * seq_count, seq_count, 0)
    expert_ids = jnp.arange(groups, dtype=jnp.int32)
    chosen = (my_routes[:, None] == expert_ids[None, :]).astype(jnp.int32)
    ranking = jnp.sum((jnp.cumsum(chosen, axis=0) - chosen) * chosen, axis=1)
    slot_ids = jnp.arange(capacity, dtype=jnp.int32)
    placed = (chosen[:, :, None] * (ranking[:, None, None] == slot_ids[None, None, :])).astype(
        jnp.float32
    )
    placed = placed.reshape(seq_count, top_count, groups * capacity)
    selector = jnp.sum(placed, axis=1)
    combine_weights = jnp.sum(placed * my_weights[:, :, None], axis=1)
    outgoing = jnp.dot(
        selector.T.astype(jnp.bfloat16), normed_ffn, preferred_element_type=jnp.float32
    )
    outgoing = outgoing.astype(jnp.bfloat16).reshape(groups, capacity, model_width)
    block = lax.all_to_all(outgoing, "ep", split_axis=0, concat_axis=0, tiled=True)
    item_count = block.shape[1]
    answered = expert_rows(
        block.reshape(-1, model_width), w_expert_gate, w_expert_up, expert_down_weight
    )
    answered = answered.reshape(groups, item_count, slice_width)
    returned = lax.all_to_all(answered, "ep", split_axis=0, concat_axis=0, tiled=True)
    expert_out = returned.reshape(groups * capacity, slice_width).astype(jnp.float32)
    combined = jnp.dot(combine_weights, expert_out, preferred_element_type=jnp.float32)
    return (own_stream.astype(jnp.float32) + combined).astype(jnp.bfloat16)


def solution(mesh):
    placed = (
        P("ep", None),
        P(),
        P("ep", "tp"),
        P("ep", "tp"),
        P("ep", "tp"),
        P(),
        P(),
        P("ep", None, "tp"),
        P("ep", None, "tp"),
        P("ep", "tp", None),
        P("ep"),
        P("tp", None),
        P(),
        P(),
        P(),
        P("ep", None, "tp"),
        P("ep", None, "tp"),
        P("ep", "tp", None),
    )
    return jax.shard_map(
        shards, mesh=mesh, in_specs=placed, out_specs=P("ep", "tp"), check_vma=False
    )
```

profile of v0, /device:TPU:1, one launch (start us, length us, event | category | flops | bytes accessed | tf_op | source)
XLA Modules:
  0.0 120.6 jit_solution(13331741680756361450)
XLA Ops:
  0.0 0.0 copy-start
  0.0 0.0 copy-start.6
  0.0 0.0 copy-start.4
  0.0 1.1 fusion.21
  1.1 1.6 %copy_bitcast_fusion = bf16[16,16,128]{2,0,1:T(8,128)(2,1)} fusion(f32[2048]{0:T(1024)} %param.19, f32[16]{0:T(128)S(1)} %add_rsqrt_fusion.1, bf16[16,2048]{1,0:T(8,128)(2,1)} %param.18), kind=kLoop, calls=%fused_computation.43 | loop fusion | flops 131072 | bytes 139328 | tf_op jit(solution)/shard_map/all_to_all | solution.py:78
  2.7 7.6 %all-to-all-start = ((bf16[16,16,128]{2,0,1:T(8,128)(2,1)}), bf16[16,16,128]{2,0,1:T(8,128)(2,1)S(1)}, u32[]{:S(2)}, u32[]{:S(2)}) async-start(bf16[16,16,128]{2,0,1:T(8,128)(2,1)} %copy_bitcast_fusion), calls=%async_computation | async-start | bytes 131072 | tf_op jit(solution)/shard_map/all_to_all | solution.py:78
  10.3 1.1 fusion.69
  11.4 5.4 %all-to-all-done = bf16[16,16,128]{2,0,1:T(8,128)(2,1)S(1)} async-done(((bf16[16,16,128]{2,0,1:T(8,128)(2,1)}), bf16[16,16,128]{2,0,1:T(8,128)(2,1)S(1)}, u32[]{:S(2)}, u32[]{:S(2)}) %all-to-all-start) | async-done | bytes 65568 | tf_op jit(solution)/shard_map/all_to_all | solution.py:78
  16.8 1.7 %fusion.25 = f32[16,16,384]{2,1,0:T(8,128)} fusion(bf16[128,128]{1,0:T(8,128)(2,1)} %param.22, bf16[128,128]{1,0:T(8,128)(2,1)} %param.21, bf16[128,128]{1,0:T(8,128)(2,1)} %param.20, bf16[16,16,128]{2,0,1:T(8,128)(2,1)S(1)} %all-to-all-done), kind=kOutput, calls=%fused_computation.33 | convolution fusion | flops 25460736 | bytes 557056 | tf_op jit(solution)/shard_map/dot_general | solution.py:81
  18.5 3.6 %all-to-all-start.1 = ((f32[16,16,384]{2,1,0:T(8,128)}), f32[16,16,384]{2,1,0:T(8,128)S(1)}, u32[]{:S(2)}, u32[]{:S(2)}) async-start(f32[16,16,384]{2,1,0:T(8,128)} %fusion.25), calls=%async_computation.1 | async-start | bytes 786432 | tf_op jit(solution)/shard_map/all_to_all | solution.py:20
  22.1 0.0 copy-done.6
  22.1 0.0 copy-done.4
  22.1 0.3 fusion.45
  22.4 8.1 %all-to-all-done.1 = f32[16,16,384]{2,1,0:T(8,128)S(1)} async-done(((f32[16,16,384]{2,1,0:T(8,128)}), f32[16,16,384]{2,1,0:T(8,128)S(1)}, u32[]{:S(2)}, u32[]{:S(2)}) %all-to-all-start.1) | async-done | bytes 393248 | tf_op jit(solution)/shard_map/all_to_all | solution.py:20
  30.6 0.1 fusion.52
  30.7 0.0 copy-start.9
  30.7 3.5 %fusion.53 = f32[16,1,1024]{2,1,0:T(1,128)S(1)} fusion(bf16[16,1024,128]{2,1,0:T(8,128)(2,1)} %param.25, bf16[16,128,1]{1,0,2:T(8,128)(2,1)S(1)} %slice_bitcast_fusion), kind=kOutput, calls=%fused_computation.67 | convolution fusion | flops 4194304 | bytes 4263936 | tf_op jit(solution)/shard_map/shd,sphd->shp/dot_general | solution.py:110
  34.2 0.1 fusion.39
  34.3 0.3 fusion.68
  34.6 0.3 fusion.65
  35.0 0.0 copy-done.9
  35.0 0.0 copy-start.3
  35.0 0.7 fusion.36
  35.7 0.3 copy-done.3
  36.0 0.2 convolution_convert_fusion.2
  36.3 0.0 copy-start.7
  36.3 1.1 broadcast_in_dim.11
  37.4 0.0 copy-start.8
  37.4 11.6 %all-to-all-start.2 = ((bf16[16,16,2048]{2,1,0:T(8,128)(2,1)}), bf16[16,16,2048]{2,1,0:T(8,128)(2,1)S(1)}, u32[]{:S(2)}, u32[]{:S(2)}) async-start(bf16[16,16,2048]{2,1,0:T(8,128)(2,1)} %broadcast_in_dim.11), calls=%async_computation.2 | async-start | bytes 2097152 | tf_op jit(solution)/shard_map/all_to_all | solution.py:26
  49.0 0.0 copy-start.5
  49.0 0.0 copy-done.7
  49.0 0.1 constant_dynamic-slice_fusion.2
  49.1 0.1 copy.29
  49.2 0.1 eq.58
  49.3 0.1 fusion.48
  49.4 0.1 reduce_window_sum.11
  49.4 0.2 select_reduce_fusion
  49.6 0.1 fusion.49
  49.7 0.1 multiply_convert_fusion
  49.8 0.2 convert_element_type.100
  50.0 0.0 copy-done.8
  50.0 0.1 constant_dynamic-slice_fusion
  50.1 0.1 copy.30
  50.2 0.1 fusion.66
  50.3 26.7 %all-to-all-done.2 = bf16[16,16,2048]{2,1,0:T(8,128)(2,1)S(1)} async-done(((bf16[16,16,2048]{2,1,0:T(8,128)(2,1)}), bf16[16,16,2048]{2,1,0:T(8,128)(2,1)S(1)}, u32[]{:S(2)}, u32[]{:S(2)}) %all-to-all-start.2) | async-done | bytes 1048608 | tf_op jit(solution)/shard_map/all_to_all | solution.py:26
  77.0 0.1 convert_reduce_fusion
  77.1 0.0 copy-done.2
  77.1 0.0 copy-start.1
  77.2 0.1 fusion.18
  77.3 0.0 copy-done.5
  77.3 0.3 convolution_convert_fusion.1
  77.6 0.1 reshape.220
  77.7 11.3 %all_to_all.41 = bf16[16,4,2048]{2,1,0:T(4,128)(2,1)} all-to-all(bf16[16,4,2048]{2,1,0:T(4,128)(2,1)S(1)} %reshape.220), channel_id=1, replica_groups=mesh['ep'=16,'tp'=16] {'ep'}, dimensions={0} | all-to-all | bytes 524288 | tf_op jit(solution)/shard_map/all_to_all | solution.py:150
  89.0 1.0 reshape.221
  90.0 0.0 copy-done.1
  90.0 0.6 fusion.3
  90.6 0.0 copy-done
  90.6 2.6 %fusion.5 = bf16[8,16,8,128]{3,2,1,0:T(8,128)(2,1)S(1)} fusion(bf16[1,352,2048]{2,1,0:T(8,128)(2,1)S(1)} %copy-done, bf16[64,2048]{1,0:T(8,128)(2,1)S(1)} %reshape.221, bf16[1,2048,352]{1,2,0:T(8,128)(2,1)} %param.34, f32[64,352]{1,0:T(8,128)S(1)} %fusion.3), kind=kOutput, calls=%fused_computation.9 | convolution fusion | flops 184815616 | bytes 3497984 | tf_op jit(solution)/shard_map/dot_general | solution.py:44
  93.1 0.1 copy.47
  93.2 16.0 %all_to_all.42 = bf16[16,64,128]{2,1,0:T(8,128)(2,1)S(1)} all-to-all(bf16[16,64,128]{2,1,0:T(8,128)(2,1)S(1)} %bitcast.67), channel_id=1, replica_groups=mesh['ep'=16,'tp'=16] {'tp'}, dimensions={0} | all-to-all | bytes 524288 | tf_op jit(solution)/shard_map/all_to_all | solution.py:14
  109.2 0.6 reduce_sum.102
  109.9 3.5 %all-to-all-start.5 = ((bf16[16,4,128]{2,1,0:T(4,128)(2,1)}), bf16[16,4,128]{2,1,0:T(4,128)(2,1)S(1)}, u32[]{:S(2)}, u32[]{:S(2)}) async-start(bf16[16,4,128]{2,1,0:T(4,128)(2,1)} %bitcast.14), calls=%async_computation.5 | async-start | bytes 32768 | tf_op jit(solution)/shard_map/all_to_all | solution.py:156
  113.4 6.5 %all-to-all-done.5 = bf16[16,4,128]{2,1,0:T(4,128)(2,1)S(1)} async-done(((bf16[16,4,128]{2,1,0:T(4,128)(2,1)}), bf16[16,4,128]{2,1,0:T(4,128)(2,1)S(1)}, u32[]{:S(2)}, u32[]{:S(2)}) %all-to-all-start.5) | async-done | bytes 16416 | tf_op jit(solution)/shard_map/all_to_all | solution.py:156
  119.9 0.7 fusion.15
  (10 shorter events, 0.1 us)
Async XLA Ops:
  0.0 90.6 %copy-start = (bf16[1,352,2048]{2,1,0:T(8,128)(2,1)S(1)}, bf16[1,352,2048]{2,1,0:T(8,128)(2,1)}, u32[]{:S(2)}) copy-start(bf16[1,352,2048]{2,1,0:T(8,128)(2,1)} %param.35) | copy-start | bytes 4325380
  0.0 22.1 %copy-start.6 = (s32[16]{0:T(128)S(1)}, s32[16]{0:T(128)}, u32[]{:S(2)}) copy-start(s32[16]{0:T(128)} %param.28) | copy-start | bytes 196
  0.0 22.1 %copy-start.4 = (f32[16,1,1024]{2,1,0:T(1,128)S(1)}, f32[16,1,1024]{2,1,0:T(1,128)}, u32[]{:S(2)}) copy-start(f32[16,1,1024]{2,1,0:T(1,128)} %param.27) | copy-start | bytes 196612
  2.7 14.1 %all-to-all-start = ((bf16[16,16,128]{2,0,1:T(8,128)(2,1)}), bf16[16,16,128]{2,0,1:T(8,128)(2,1)S(1)}, u32[]{:S(2)}, u32[]{:S(2)}) async-start(bf16[16,16,128]{2,0,1:T(8,128)(2,1)} %copy_bitcast_fusion), calls=%async_computation | async-start | bytes 131072 | tf_op jit(solution)/shard_map/all_to_all | solution.py:78
  18.5 12.0 %all-to-all-start.1 = ((f32[16,16,384]{2,1,0:T(8,128)}), f32[16,16,384]{2,1,0:T(8,128)S(1)}, u32[]{:S(2)}, u32[]{:S(2)}) async-start(f32[16,16,384]{2,1,0:T(8,128)} %fusion.25), calls=%async_computation.1 | async-start | bytes 786432 | tf_op jit(solution)/shard_map/all_to_all | solution.py:20
  30.7 4.3 %copy-start.9 = (bf16[16,1024,128]{2,1,0:T(8,128)(2,1)S(1)}, bf16[16,1024,128]{2,1,0:T(8,128)(2,1)}, u32[]{:S(2)}) copy-start(bf16[16,1024,128]{2,1,0:T(8,128)(2,1)} %param.26) | copy-start | bytes 12582916
  35.0 1.0 copy-start.3
  36.3 12.8 %copy-start.7 = (s32[256,2]{0,1:T(2,128)S(1)}, s32[256,2]{0,1:T(2,128)}, u32[]{:S(2)}) copy-start(s32[256,2]{0,1:T(2,128)} %param.31) | copy-start | bytes 6148
  37.4 12.6 %copy-start.8 = (f32[256,2]{0,1:T(2,128)S(1)}, f32[256,2]{0,1:T(2,128)}, u32[]{:S(2)}) copy-start(f32[256,2]{0,1:T(2,128)} %param.32) | copy-start | bytes 6148
  37.4 39.6 %all-to-all-start.2 = ((bf16[16,16,2048]{2,1,0:T(8,128)(2,1)}), bf16[16,16,2048]{2,1,0:T(8,128)(2,1)S(1)}, u32[]{:S(2)}, u32[]{:S(2)}) async-start(bf16[16,16,2048]{2,1,0:T(8,128)(2,1)} %broadcast_in_dim.11), calls=%async_computation.2 | async-start | bytes 2097152 | tf_op jit(solution)/shard_map/all_to_all | solution.py:26
  49.0 28.1 %copy-start.2 = (bf16[16,2048]{1,0:T(8,128)(2,1)S(1)}, bf16[16,2048]{1,0:T(8,128)(2,1)}, u32[]{:S(2)}) copy-start(bf16[16,2048]{1,0:T(8,128)(2,1)} %param.18) | copy-start | bytes 196612
  49.0 28.3 %copy-start.5 = (f32[2048]{0:T(1024)S(1)}, f32[2048]{0:T(1024)}, u32[]{:S(2)}) copy-start(f32[2048]{0:T(1024)} %param.30) | copy-start | bytes 24580
  77.1 12.8 %copy-start.1 = (bf16[1,2048,352]{1,2,0:T(8,128)(2,1)S(1)}, bf16[1,2048,352]{1,2,0:T(8,128)(2,1)}, u32[]{:S(2)}) copy-start(bf16[1,2048,352]{1,2,0:T(8,128)(2,1)} %param.33) | copy-start | bytes 4325380
  109.9 10.0 %all-to-all-start.5 = ((bf16[16,4,128]{2,1,0:T(4,128)(2,1)}), bf16[16,4,128]{2,1,0:T(4,128)(2,1)S(1)}, u32[]{:S(2)}, u32[]{:S(2)}) async-start(bf16[16,4,128]{2,1,0:T(4,128)(2,1)} %bitcast.14), calls=%async_computation.5 | async-start | bytes 32768 | tf_op jit(solution)/shard_map/all_to_all | solution.py:156
where the time goes:
time: 121 us
  waiting for transfers between devices  46.7 us (39%)
  blocking collectives  27.3 us (23%)
  starting transfers between devices  26.2 us (22%)
  matrix products  11.4 us (9%)
  other arithmetic  5.47 us (5%)
  local copies, waits for them, and re-layouts  3.24 us (3%)
    all_to_all x1, waiting for transfers between devices, from_everyone(): return lax.all_to_all(copies, axis, split_axis=0, concat_axis=0, tiled=True)  26.7 us
    all_to_all x1, blocking collectives, sent_and_summed(): blocks = lax.all_to_all(split_up(shard, dim, peers), axis, 0, 0, tiled=True)  16 us
    all_to_all x1, starting transfers between devices, from_everyone(): return lax.all_to_all(copies, axis, split_axis=0, concat_axis=0, tiled=True)  11.6 us
    all_to_all x1, blocking collectives, shards(): lax.all_to_all(outgoing, 'ep', split_axis=0, concat_axis=0, tiled=True)  11.3 us
    all_to_all x1, waiting for transfers between devices, sum_at_owner(): lax.all_to_all(blocks, axis, split_axis=0, concat_axis=0, tiled=True)  8.1 us
    all_to_all x1, starting transfers between devices, shards(): lax.all_to_all(normed, 'ep', split_axis=1, concat_axis=0, tiled=True)  7.57 us
    all_to_all x1, waiting for transfers between devices, shards(): lax.all_to_all(answered, 'ep', split_axis=0, concat_axis=0, tiled=True)  6.48 us
    all_to_all x1, waiting for transfers between devices, shards(): lax.all_to_all(normed, 'ep', split_axis=1, concat_axis=0, tiled=True)  5.41 us
  transfers between devices with their start and end apart: 4, of which 4 were waited for; matrix products, arithmetic and copies ran while one was open for 2% of the time, Pallas kernels for 0%

commit v1 on v0

v1 whole, which is shorter than its diff:
```python
import functools

import jax
import jax.numpy as jnp
from jax import lax
from jax.experimental import pallas as pl
from jax.experimental.pallas import tpu as pltpu
from jax.sharding import PartitionSpec as P

MESH = pl.DeviceIdType.MESH
F32, BF16 = jnp.float32, jnp.bfloat16
NN = (((1,), (0,)), ((), ()))
NT = (((1,), (1,)), ((), ()))


def mm(a, b, dims=NN):
    return lax.dot_general(a, b, dims, preferred_element_type=F32)


def iota(shape, dim):
    return lax.broadcasted_iota(jnp.int32, shape, dim)


def ep_peer(me, i, n):
    if n != 16:
        return lax.rem(me + 1 + i, n)
    o = jnp.where(i < 11, 11 - i, 26 - i)
    y = lax.rem(me // 4 + o // 4, 4)
    x = lax.rem(lax.rem(me, 4) + lax.rem(o, 4), 4)
    return y * 4 + x


def tp_peer(me, i, n):
    half = (i + 1) // 2
    o = n // 2 + jnp.where(lax.rem(i, 2) == 1, -half, half)
    return lax.rem(me + o, n)


def kernel(
    cfg,
    stream_h, gain1_h, wq_h, wk_h, wv_h, wf_h, fb_h, kc_h, vc_h, gc_h, len_h,
    wo_h, gain2_h, rt_h, rw_h, wg_h, wu_h, wd_h,
    out_ref,
    stream, gain1, wqkv, wf, fb, kc, vc, gc, lens, wo, gain2, rt, rw, wg, wu, wd,
    xn, xin, qs, kvs, qr, kvr, os_, or_, mx, mxr, ss, sr, es, er, fs, fr,
    pick, unpick, spread, comb,
    load_sem, send_sem, recv_sem,
):
    ne, nt, cap = cfg
    seqs, width = stream.shape
    blk = width // ne
    slc = width // nt
    cache = kc.shape[1]
    hd = kc.shape[2]
    parts = 16 // cap
    cw = width // parts
    g = lax.axis_index("ep")
    t = lax.axis_index("tp")

    barrier = pltpu.get_barrier_semaphore()

    def greet_ep(i, c):
        pl.semaphore_signal(barrier, inc=1, device_id={"ep": ep_peer(g, i, ne)}, device_id_type=MESH)
        return c

    def greet_tp(i, c):
        pl.semaphore_signal(barrier, inc=1, device_id={"tp": tp_peer(t, i, nt)}, device_id_type=MESH)
        return c

    lax.fori_loop(0, ne - 1, greet_ep, 0)
    lax.fori_loop(0, nt - 1, greet_tp, 0)

    loads = [
        (stream_h, stream), (gain1_h, gain1),
        (wq_h, wqkv.at[:, pl.ds(0, hd)]), (wk_h, wqkv.at[:, pl.ds(hd, hd)]),
        (wv_h, wqkv.at[:, pl.ds(2 * hd, hd)]),
        (wf_h, wf), (fb_h, fb), (len_h, lens), (rt_h, rt), (rw_h, rw), (gc_h, gc),
        (kc_h, kc), (wo_h, wo), (vc_h, vc), (gain2_h, gain2),
        (wg_h.at[0], wg), (wu_h.at[0], wu), (wd_h.at[0], wd),
    ]
    copies = [pltpu.make_async_copy(a, b, load_sem.at[i]) for i, (a, b) in enumerate(loads)]
    for c in copies:
        c.start()
    (c_stream, c_gain1, c_q, c_k, c_v, c_wf, c_fb, c_len, c_rt, c_rw, c_gc,
     c_kc, c_wo, c_vc, c_gain2, c_wg, c_wu, c_wd) = copies

    def remote(src, dst, phase, where):
        return pltpu.make_async_remote_copy(
            src_ref=src, dst_ref=dst, send_sem=send_sem.at[phase], recv_sem=recv_sem.at[phase],
            device_id=where, device_id_type=MESH)

    def send_ep(pairs):
        def body(i, c):
            peer = ep_peer(g, i, ne)
            for src, dst, phase in pairs:
                remote(src.at[peer], dst.at[g], phase, {"ep": peer}).start()
            return c
        lax.fori_loop(0, ne - 1, body, 0)

    def send_tp(src, dst, phase, whole=False):
        def body(i, c):
            peer = tp_peer(t, i, nt)
            remote(src if whole else src.at[peer], dst.at[t], phase, {"tp": peer}).start()
            return c
        lax.fori_loop(0, nt - 1, body, 0)

    def arrived(buf, phase, axis, n):
        part = buf.at[pl.ds(0, n - 1)]
        remote(part, part, phase, {axis: 0}).wait_recv()

    def gone(buf, phase, axis, n):
        part = buf.at[pl.ds(0, n - 1)]
        remote(part, part, phase, {axis: 0}).wait_send()

    c_stream.wait()
    c_gain1.wait()
    xf = stream[...].astype(F32)
    rs = lax.rsqrt(jnp.mean(xf * xf, axis=-1, keepdims=True) + 1e-06)
    normed = (xf * rs * gain1[...]).astype(BF16)
    for b in range(ne):
        xn[b] = normed[:, b * blk:(b + 1) * blk]
    pl.semaphore_wait(barrier, ne + nt - 2)
    send_ep([(xn, xin, 0)])
    xin[g] = xn[g]

    c_wf.wait()
    c_fb.wait()
    fz = mm(normed, wf[...], NT) + fb[...]
    heads = fz.shape[1]
    z = jnp.sum(jnp.where(iota(fz.shape, 1) == t, fz, 0.0), axis=1, keepdims=True)
    forget = jnp.minimum(z, 0.0) - jnp.log1p(jnp.exp(-jnp.abs(z)))

    c_len.wait()
    lsq = iota((seqs, seqs), 0) == iota((seqs, seqs), 1)
    length = jnp.sum(jnp.where(lsq, lens[...].astype(F32), 0.0), axis=1, keepdims=True).astype(jnp.int32)
    c_gc.wait()
    row = iota((seqs, cache), 0)
    pos = iota((seqs, cache), 1)
    gates = jnp.zeros((seqs, cache), F32)
    for s in range(seqs):
        gates = jnp.where(row == s, gc[s], gates)
    live = pos < length
    last_gate = jnp.sum(jnp.where(pos == length - 1, gates, 0.0), axis=1, keepdims=True)

    c_rt.wait()
    c_rw.wait()
    batch = rt.shape[1]
    mine = iota((seqs, batch), 1) == g * seqs + iota((seqs, batch), 0)
    lanes = ne * 16
    lane = iota((seqs, lanes), 1)
    lane_e, lane_j, lane_r = lane // 16, lax.rem(lane // cap, parts), lax.rem(lane, cap)
    chosen = jnp.zeros((seqs, lanes), F32)
    weight = jnp.zeros((seqs, lanes), F32)
    for k in range(rt.shape[0]):
        rk = jnp.sum(jnp.where(mine, rt[k:k + 1, :].astype(F32), 0.0), axis=1, keepdims=True).astype(jnp.int32)
        wk_ = jnp.sum(jnp.where(mine, rw[k:k + 1, :], 0.0), axis=1, keepdims=True)
        hit = rk == lane_e
        chosen = chosen + jnp.where(hit, 1.0, 0.0)
        weight = weight + jnp.where(hit, wk_, 0.0)
    before = (iota((seqs, seqs), 1) < iota((seqs, seqs), 0)).astype(F32).astype(BF16)
    rank = mm(before, chosen.astype(BF16))
    slot = rank == lane_r.astype(F32)
    chosen = jnp.where(slot, chosen, 0.0)
    weight = jnp.where(slot, weight, 0.0)
    w_hi = weight.astype(BF16)
    w_lo = (weight - w_hi.astype(F32)).astype(BF16)
    picked = []
    for j in range(parts):
        here = lane_j == j
        picked.append(jnp.where(here, chosen, 0.0))
        zero = jnp.zeros_like(w_hi)
        comb[pl.ds(2 * j * seqs, seqs), :] = jnp.where(here, w_hi.astype(F32), 0.0).astype(BF16)
        comb[pl.ds((2 * j + 1) * seqs, seqs), :] = jnp.where(here, w_lo.astype(F32), 0.0).astype(BF16)
    pick[...] = jnp.concatenate(picked, axis=0).T.astype(BF16)

    rows = ne * cap
    a, b = iota((parts * rows, lanes), 0), iota((parts * rows, lanes), 1)
    same = (a // rows == lax.rem(b // cap, parts)) & (lax.rem(a, rows) // cap == b // 16) & (lax.rem(a, cap) == lax.rem(b, cap))
    unpick[...] = jnp.where(same, 1.0, 0.0).astype(BF16)
    a, b = iota((lanes, parts * rows), 1), iota((lanes, parts * rows), 0)
    same = (a // rows == lax.rem(b // cap, parts)) & (lax.rem(a, rows) // cap == b // 16) & (lax.rem(a, cap) == lax.rem(b, cap))
    spread[...] = jnp.where(same, 1.0, 0.0).astype(BF16)

    c_q.wait()
    c_k.wait()
    c_v.wait()
    arrived(xin, 0, "ep", ne)
    proj = mm(xin[...].reshape(ne * seqs, blk), wqkv[...])
    qs[...] = proj[:, :hd].reshape(ne, seqs, hd)
    kvs[...] = proj[:, hd:].astype(BF16).reshape(ne, seqs, 2 * hd)
    send_ep([(qs, qr, 1), (kvs, kvr, 2)])
    qr[g] = qs[g]
    kvr[g] = kvs[g]
    arrived(qr, 1, "ep", ne)
    arrived(kvr, 2, "ep", ne)
    query = jnp.sum(qr[...], axis=0).astype(BF16)
    kv = jnp.sum(kvr[...].astype(F32), axis=0).astype(BF16)
    key_new, value_new = kv[:, :hd], kv[:, hd:]

    scale = hd ** (-0.5)
    c_kc.wait()
    scores = jnp.zeros((seqs, cache), F32)
    for s in range(seqs):
        scores = jnp.where(row == s, mm(query, kc[s], NT), scores)
    scores = scores * scale + forget + last_gate - gates
    scores = jnp.where(live, scores, -1e30)
    own = jnp.sum(query.astype(F32) * key_new.astype(F32), axis=1, keepdims=True) * scale
    top = jnp.maximum(jnp.max(scores, axis=1, keepdims=True), own)
    past = jnp.exp(scores - top)
    own = jnp.exp(own - top)
    total = jnp.sum(past, axis=1, keepdims=True) + own
    past = (past / total).astype(BF16)
    own = (own / total).astype(BF16)
    c_vc.wait()
    hrow = iota((seqs, hd), 0)
    att = jnp.zeros((seqs, hd), F32)
    for s in range(seqs):
        att = jnp.where(hrow == s, mm(past, vc[s]), att)
    att = (att + own.astype(F32) * value_new.astype(F32)).astype(BF16)

    c_wo.wait()
    share = mm(att, wo[...]).astype(BF16)
    for u in range(nt):
        os_[u] = share[:, u * slc:(u + 1) * slc]
    send_tp(os_, or_, 3)
    or_[t] = os_[t]
    own_stream = stream[:, pl.ds(pl.multiple_of(t * slc, slc), slc)].astype(F32)
    arrived(or_, 3, "tp", nt)
    mixed = (own_stream + jnp.sum(or_[...].astype(F32), axis=0)).astype(BF16)
    mx[...] = mixed
    send_tp(mx, mxr, 4, whole=True)
    mxr[t] = mixed
    arrived(mxr, 4, "tp", nt)

    per = nt // parts
    stacked = jnp.concatenate(
        [jnp.concatenate([mxr[j * per + u] for u in range(per)], axis=1) for j in range(parts)], axis=0)
    ss[...] = mm(pick[...], stacked).astype(BF16).reshape(ne, 16, cw)
    send_ep([(ss, sr, 5)])
    sr[g] = ss[g]
    c_gain2.wait()
    c_wg.wait()
    c_wu.wait()
    arrived(sr, 5, "ep", ne)
    rows_in = mm(unpick[...], sr[...].reshape(lanes, cw))
    xs = jnp.concatenate([rows_in[j * rows:(j + 1) * rows] for j in range(parts)], axis=1)
    rs2 = lax.rsqrt(jnp.mean(xs * xs, axis=-1, keepdims=True) + 1e-06)
    xs = (xs * rs2 * gain2[...]).astype(BF16)
    gate = mm(xs, wg[...], NT)
    up = mm(xs, wu[...], NT)
    hidden = (gate / (1.0 + jnp.exp(-gate)) * up).astype(BF16)
    c_wd.wait()
    part = mm(hidden, wd[...]).astype(BF16)
    part = jnp.concatenate([part[:, j * cw:(j + 1) * cw] for j in range(parts)], axis=0)
    es[...] = mm(spread[...], part).astype(BF16).reshape(ne, 16, cw)
    send_ep([(es, er, 6)])
    er[g] = es[g]
    arrived(er, 6, "ep", ne)

    both = mm(comb[...], er[...].reshape(lanes, cw))
    for j in range(parts):
        piece = (both[2 * j * seqs:(2 * j + 1) * seqs] + both[(2 * j + 1) * seqs:(2 * j + 2) * seqs]).astype(BF16)
        for u in range(per):
            fs[j * per + u] = piece[:, u * slc:(u + 1) * slc]
    send_tp(fs, fr, 7)
    fr[t] = fs[t]
    arrived(fr, 7, "tp", nt)
    out_ref[...] = (mixed.astype(F32) + jnp.sum(fr[...].astype(F32), axis=0)).astype(BF16)

    for buf, phase, axis, n in (
        (xin, 0, "ep", ne), (qr, 1, "ep", ne), (kvr, 2, "ep", ne), (or_, 3, "tp", nt),
        (mxr, 4, "tp", nt), (sr, 5, "ep", ne), (er, 6, "ep", ne), (fr, 7, "tp", nt)):
        gone(buf, phase, axis, n)


def shards(
    ne, nt, stream, norm_gain_attn, w_query, w_key, w_value, w_forget, forget_bias,
    key_cache, value_cache, gate_cache, lengths, w_output, norm_gain_ffn,
    routes, route_weights, w_expert_gate, w_expert_up, expert_down_weight,
):
    seqs, width = stream.shape
    cache, hd = key_cache.shape[1:]
    tops = routes.shape[1]
    cap = 2 * seqs * tops // ne
    blk, slc, hid = width // ne, width // nt, w_expert_gate.shape[2]
    parts = 16 // cap
    cw = width // parts
    args = (
        stream, norm_gain_attn.reshape(1, -1), w_query, w_key, w_value, w_forget.T,
        forget_bias.reshape(1, -1), key_cache, value_cache, gate_cache, lengths.reshape(1, -1),
        w_output, norm_gain_ffn.reshape(1, -1), routes.T, route_weights.T,
        jnp.swapaxes(w_expert_gate, 1, 2), jnp.swapaxes(w_expert_up, 1, 2), expert_down_weight,
    )
    V = pltpu.VMEM
    scratch = [
        V((seqs, width), BF16), V((1, width), F32), V((blk, 3 * hd), BF16),
        V(w_forget.shape[::-1], BF16), V((1, forget_bias.shape[0]), F32),
        V(key_cache.shape, BF16), V(value_cache.shape, BF16), V(gate_cache.shape, F32),
        V((1, seqs), jnp.int32), V(w_output.shape, BF16), V((1, width), F32),
        V(routes.shape[::-1], jnp.int32), V(routes.shape[::-1], F32),
        V((hid, width), BF16), V((hid, width), BF16), V((hid, width), BF16),
        V((ne, seqs, blk), BF16), V((ne, seqs, blk), BF16),
        V((ne, seqs, hd), F32), V((ne, seqs, 2 * hd), BF16),
        V((ne, seqs, hd), F32), V((ne, seqs, 2 * hd), BF16),
        V((nt, seqs, slc), BF16), V((nt, seqs, slc), BF16),
        V((seqs, slc), BF16), V((nt, seqs, slc), BF16),
        V((ne, 16, cw), BF16), V((ne, 16, cw), BF16),
        V((ne, 16, cw), BF16), V((ne, 16, cw), BF16),
        V((nt, seqs, slc), BF16), V((nt, seqs, slc), BF16),
        V((ne * 16, parts * seqs), BF16), V((parts * ne * cap, ne * 16), BF16),
        V((ne * 16, parts * ne * cap), BF16), V((2 * parts * seqs, ne * 16), BF16),
        pltpu.SemaphoreType.DMA((18,)), pltpu.SemaphoreType.DMA((8,)), pltpu.SemaphoreType.DMA((8,)),
    ]
    return pl.pallas_call(
        functools.partial(kernel, (ne, nt, cap)),
        out_shape=jax.ShapeDtypeStruct((seqs, slc), BF16),
        in_specs=[pl.BlockSpec(memory_space=pl.ANY)] * len(args),
        out_specs=pl.BlockSpec(memory_space=pltpu.VMEM),
        scratch_shapes=scratch,
        compiler_params=pltpu.CompilerParams(
            collective_id=0, has_side_effects=True, vmem_limit_bytes=48 * 1024 * 1024),
        name="layer",
    )(*args)


def solution(mesh):
    placed = (
        P("ep", None), P(), P("ep", "tp"), P("ep", "tp"), P("ep", "tp"), P(), P(),
        P("ep", None, "tp"), P("ep", None, "tp"), P("ep", "tp", None), P("ep"),
        P("tp", None), P(), P(), P(),
        P("ep", None, "tp"), P("ep", None, "tp"), P("ep", "tp", None),
    )
    return jax.shard_map(
        functools.partial(shards, mesh.shape["ep"], mesh.shape["tp"]),
        mesh=mesh, in_specs=placed, out_specs=P("ep", "tp"), check_vma=False,
    )
```

time: 121 us -> 66.2 us (0.55)
  Pallas kernels: 0 us -> 50.9 us
  waiting for transfers between devices: 46.7 us -> 0 us
  blocking collectives: 27.3 us -> 0 us
  starting transfers between devices: 26.2 us -> 0 us
  matrix products: 11.4 us -> 0 us
  local copies, waits for them, and re-layouts: 3.24 us -> 14.6 us
  other arithmetic: 5.47 us -> 0 us
    pallas_call x0 -> x1, Pallas kernels: none -> 50.9 us  [shards(): pl.pallas_call(functools.partial(kernel, (ne, nt, cap)), out_shape=jax.Sh...]
    all_to_all x4 -> x0, waiting for transfers between devices: 46.7 us -> none  [the longest x1 26.7 us: from_everyone(): return lax.all_to_all(copies, axis, split_axis=0, concat_axis=0, tiled=True)]
    all_to_all x2 -> x0, blocking collectives: 27.3 us -> none  [the longest x1 16 us: sent_and_summed(): blocks = lax.all_to_all(split_up(shard, dim, peers), axis, 0, 0, tiled=True)]
    all_to_all x4 -> x0, starting transfers between devices: 26.2 us -> none  [the longest x1 11.6 us: from_everyone(): return lax.all_to_all(copies, axis, split_axis=0, concat_axis=0, tiled=True)]
    unnamed x20 -> x33, local copies, waits for them, and re-layouts: 0.36 us -> 14.6 us
    dot_general x9 -> x0, matrix products: 11.4 us -> none  [the longest x1 3.52 us: shards(): jnp.einsum('shd,sphd->shp', query, keys, preferred_element_type=jnp.float32)]
    reduce_sum x9 -> x0, other arithmetic: 2.96 us -> none  [the longest x2 1.22 us: rms_norm(): jnp.mean(floats * floats, axis=-1, keepdims=True) + 1e-06]
    all_to_all x1 -> x0, other arithmetic: 1.57 us -> none  [shards(): lax.all_to_all(normed, 'ep', split_axis=1, concat_axis=0, tiled=True)]
  transfers between devices with their start and end apart: 4 -> 0, of which waited for: 4 -> 0; matrix products, arithmetic and copies ran while one was open for 2% -> 0% of each run, Pallas kernels for 0% -> 0%
where the time goes in v1:
time: 66.2 us; the launch traced here: 65.5 us
  Pallas kernels  50.9 us (77%)
  local copies, waits for them, and re-layouts  14.6 us (22%)
    pallas_call x1, Pallas kernels, shards(): pl.pallas_call(functools.partial(kernel, (ne, nt, cap)), out_shape=jax.Sh...  50.9 us
    unnamed x33, local copies, waits for them, and re-layouts  14.6 us

profile of v1, /device:TPU:1, one launch (start us, length us, event | category | flops | bytes accessed | tf_op | source)
XLA Modules:
  0.0 65.5 jit_solution(9416603628996645637)
XLA Ops:
  0.0 0.0 copy-start
  0.0 1.4 %copy-done = bf16[1,2048,352]{1,2,0:T(8,128)(2,1)S(1)} copy-done((bf16[1,2048,352]{1,2,0:T(8,128)(2,1)S(1)}, bf16[1,2048,352]{1,2,0:T(8,128)(2,1)}, u32[]{:S(2)}) %copy-start) | copy-done | bytes 1441816
  1.4 0.0 copy-start.1
  1.4 1.4 %copy-done.1 = bf16[1,2048,352]{1,2,0:T(8,128)(2,1)S(1)} copy-done((bf16[1,2048,352]{1,2,0:T(8,128)(2,1)S(1)}, bf16[1,2048,352]{1,2,0:T(8,128)(2,1)}, u32[]{:S(2)}) %copy-start.1) | copy-done | bytes 1441816
  2.7 0.0 copy-start.2
  2.7 1.4 %copy-done.2 = bf16[1,352,2048]{2,1,0:T(8,128)(2,1)S(1)} copy-done((bf16[1,352,2048]{2,1,0:T(8,128)(2,1)S(1)}, bf16[1,352,2048]{2,1,0:T(8,128)(2,1)}, u32[]{:S(2)}) %copy-start.2) | copy-done | bytes 1441816
  4.1 0.0 copy-start.3
  4.1 1.0 %copy-done.3 = bf16[128,2048]{1,0:T(8,128)(2,1)S(1)} copy-done((bf16[128,2048]{1,0:T(8,128)(2,1)S(1)}, bf16[128,2048]{1,0:T(8,128)(2,1)}, u32[]{:S(2)}) %copy-start.3) | copy-done | bytes 524312
  5.1 0.0 copy-start.4
  5.1 0.8 %copy-done.4 = bf16[16,2048]{1,0:T(8,128)(2,1)S(1)} copy-done((bf16[16,2048]{1,0:T(8,128)(2,1)S(1)}, bf16[16,2048]{1,0:T(8,128)(2,1)}, u32[]{:S(2)}) %copy-start.4) | copy-done | bytes 65560
  6.0 0.0 copy-start.5
  6.0 0.8 %copy-done.5 = bf16[2048,16]{0,1:T(8,128)(2,1)S(1)} copy-done((bf16[2048,16]{0,1:T(8,128)(2,1)S(1)}, bf16[2048,16]{0,1:T(8,128)(2,1)}, u32[]{:S(2)}) %copy-start.5) | copy-done | bytes 65560
  6.8 0.0 copy-start.6
  6.8 0.8 %copy-done.6 = f32[16,1,1024]{2,1,0:T(1,128)S(1)} copy-done((f32[16,1,1024]{2,1,0:T(1,128)S(1)}, f32[16,1,1024]{2,1,0:T(1,128)}, u32[]{:S(2)}) %copy-start.6) | copy-done | bytes 65560
  7.7 0.0 copy-start.7
  7.7 0.8 %copy-done.7 = bf16[128,128]{1,0:T(8,128)(2,1)S(1)} copy-done((bf16[128,128]{1,0:T(8,128)(2,1)S(1)}, bf16[128,128]{1,0:T(8,128)(2,1)}, u32[]{:S(2)}) %copy-start.7) | copy-done | bytes 32792
  8.4 0.0 copy-start.8
  8.4 0.8 %copy-done.8 = bf16[128,128]{1,0:T(8,128)(2,1)S(1)} copy-done((bf16[128,128]{1,0:T(8,128)(2,1)S(1)}, bf16[128,128]{1,0:T(8,128)(2,1)}, u32[]{:S(2)}) %copy-start.8) | copy-done | bytes 32792
  9.2 0.0 copy-start.9
  9.2 0.8 %copy-done.9 = bf16[128,128]{1,0:T(8,128)(2,1)S(1)} copy-done((bf16[128,128]{1,0:T(8,128)(2,1)S(1)}, bf16[128,128]{1,0:T(8,128)(2,1)}, u32[]{:S(2)}) %copy-start.9) | copy-done | bytes 32792
  9.9 0.0 copy-start.10
  9.9 0.7 %copy-done.10 = f32[2048]{0:T(1024)S(1)} copy-done((f32[2048]{0:T(1024)S(1)}, f32[2048]{0:T(1024)}, u32[]{:S(2)}) %copy-start.10) | copy-done | bytes 8216
  10.6 0.0 copy-start.11
  10.6 0.7 %copy-done.11 = f32[2048]{0:T(1024)S(1)} copy-done((f32[2048]{0:T(1024)S(1)}, f32[2048]{0:T(1024)}, u32[]{:S(2)}) %copy-start.11) | copy-done | bytes 8216
  11.3 0.0 copy-start.12
  11.3 0.7 %copy-done.12 = s32[256,2]{0,1:T(2,128)S(1)} copy-done((s32[256,2]{0,1:T(2,128)S(1)}, s32[256,2]{0,1:T(2,128)}, u32[]{:S(2)}) %copy-start.12) | copy-done | bytes 2072
  12.0 0.0 copy-start.13
  12.0 0.7 %copy-done.13 = f32[256,2]{0,1:T(2,128)S(1)} copy-done((f32[256,2]{0,1:T(2,128)S(1)}, f32[256,2]{0,1:T(2,128)}, u32[]{:S(2)}) %copy-start.13) | copy-done | bytes 2072
  12.7 0.0 copy-start.14
  12.7 0.7 copy-done.14
  13.3 0.0 copy-start.15
  13.3 0.7 copy-done.15
  14.0 50.9 %layer.1 = bf16[16,128]{1,0:T(8,128)(2,1)S(1)} custom-call(bf16[16,2048]{1,0:T(8,128)(2,1)S(1)} %copy-done.4, f32[1,2048]{1,0:T(1,128)S(1)} %bitcast.12, bf16[128,128]{1,0:T(8,128)(2,1)S(1)} %copy-done.7, bf16[128,128]{1,0:T(8,128)(2,1)S(1)} %copy-done.8, bf16[128,128]{1,0:T(8,128)(2,1)S(1)} %copy-done.9, bf16[16,2048]{1,0:T(8,128)(2,1)S(1)} %bitcast.11, ...), custom_call_target="tpu_custom_call" | custom-call | tf_op jit(solution)/shard_map/layer/pallas_call | solution.py:314
  64.9 0.6 copy.20
Async XLA Ops:
  0.0 1.4 %copy-start = (bf16[1,2048,352]{1,2,0:T(8,128)(2,1)S(1)}, bf16[1,2048,352]{1,2,0:T(8,128)(2,1)}, u32[]{:S(2)}) copy-start(bf16[1,2048,352]{1,2,0:T(8,128)(2,1)} %param.33) | copy-start | bytes 4325380
  1.4 1.4 %copy-start.1 = (bf16[1,2048,352]{1,2,0:T(8,128)(2,1)S(1)}, bf16[1,2048,352]{1,2,0:T(8,128)(2,1)}, u32[]{:S(2)}) copy-start(bf16[1,2048,352]{1,2,0:T(8,128)(2,1)} %param.34) | copy-start | bytes 4325380
  2.7 1.4 %copy-start.2 = (bf16[1,352,2048]{2,1,0:T(8,128)(2,1)S(1)}, bf16[1,352,2048]{2,1,0:T(8,128)(2,1)}, u32[]{:S(2)}) copy-start(bf16[1,352,2048]{2,1,0:T(8,128)(2,1)} %wd_h.1) | copy-start | bytes 4325380
  4.1 1.0 %copy-start.3 = (bf16[128,2048]{1,0:T(8,128)(2,1)S(1)}, bf16[128,2048]{1,0:T(8,128)(2,1)}, u32[]{:S(2)}) copy-start(bf16[128,2048]{1,0:T(8,128)(2,1)} %wo_h.1) | copy-start | bytes 1572868
  5.1 0.8 %copy-start.4 = (bf16[16,2048]{1,0:T(8,128)(2,1)S(1)}, bf16[16,2048]{1,0:T(8,128)(2,1)}, u32[]{:S(2)}) copy-start(bf16[16,2048]{1,0:T(8,128)(2,1)} %stream_h.1) | copy-start | bytes 196612
  6.0 0.8 %copy-start.5 = (bf16[2048,16]{0,1:T(8,128)(2,1)S(1)}, bf16[2048,16]{0,1:T(8,128)(2,1)}, u32[]{:S(2)}) copy-start(bf16[2048,16]{0,1:T(8,128)(2,1)} %param.23) | copy-start | bytes 196612
  6.8 0.8 %copy-start.6 = (f32[16,1,1024]{2,1,0:T(1,128)S(1)}, f32[16,1,1024]{2,1,0:T(1,128)}, u32[]{:S(2)}) copy-start(f32[16,1,1024]{2,1,0:T(1,128)} %gc_h.1) | copy-start | bytes 196612
  7.7 0.8 %copy-start.7 = (bf16[128,128]{1,0:T(8,128)(2,1)S(1)}, bf16[128,128]{1,0:T(8,128)(2,1)}, u32[]{:S(2)}) copy-start(bf16[128,128]{1,0:T(8,128)(2,1)} %wq_h.1) | copy-start | bytes 98308
  8.4 0.8 %copy-start.8 = (bf16[128,128]{1,0:T(8,128)(2,1)S(1)}, bf16[128,128]{1,0:T(8,128)(2,1)}, u32[]{:S(2)}) copy-start(bf16[128,128]{1,0:T(8,128)(2,1)} %wk_h.1) | copy-start | bytes 98308
  9.2 0.8 %copy-start.9 = (bf16[128,128]{1,0:T(8,128)(2,1)S(1)}, bf16[128,128]{1,0:T(8,128)(2,1)}, u32[]{:S(2)}) copy-start(bf16[128,128]{1,0:T(8,128)(2,1)} %wv_h.1) | copy-start | bytes 98308
  9.9 0.7 %copy-start.10 = (f32[2048]{0:T(1024)S(1)}, f32[2048]{0:T(1024)}, u32[]{:S(2)}) copy-start(f32[2048]{0:T(1024)} %param.19) | copy-start | bytes 24580
  10.6 0.7 %copy-start.11 = (f32[2048]{0:T(1024)S(1)}, f32[2048]{0:T(1024)}, u32[]{:S(2)}) copy-start(f32[2048]{0:T(1024)} %param.30) | copy-start | bytes 24580
  11.3 0.7 %copy-start.12 = (s32[256,2]{0,1:T(2,128)S(1)}, s32[256,2]{0,1:T(2,128)}, u32[]{:S(2)}) copy-start(s32[256,2]{0,1:T(2,128)} %param.31) | copy-start | bytes 6148
  12.0 0.7 %copy-start.13 = (f32[256,2]{0,1:T(2,128)S(1)}, f32[256,2]{0,1:T(2,128)}, u32[]{:S(2)}) copy-start(f32[256,2]{0,1:T(2,128)} %param.32) | copy-start | bytes 6148
  12.7 0.7 copy-start.14
  13.3 0.7 copy-start.15

commit v2 on v1

--- a/solution.py
+++ b/solution.py
@@ -21,19 +21,18 @@
     return lax.broadcasted_iota(jnp.int32, shape, dim)
 
 
-def ep_peer(me, i, n):
+def ring(me, n, size=1):
+    return [(min(o, n - o) * size, lax.rem(me + o, n)) for o in range(1, n)]
+
+
+def plane(me, n):
     if n != 16:
-        return lax.rem(me + 1 + i, n)
-    o = jnp.where(i < 11, 11 - i, 26 - i)
-    y = lax.rem(me // 4 + o // 4, 4)
-    x = lax.rem(lax.rem(me, 4) + lax.rem(o, 4), 4)
-    return y * 4 + x
-
-
-def tp_peer(me, i, n):
-    half = (i + 1) // 2
-    o = n // 2 + jnp.where(lax.rem(i, 2) == 1, -half, half)
-    return lax.rem(me + o, n)
+        return [p for _, p in sorted(ring(me, n), key=lambda q: -q[0])]
+    y, x = me // 4, lax.rem(me, 4)
+    ys = [(0, y)] + ring(y, 4)
+    xs = [(0, x)] + ring(x, 4)
+    both = [(dy + dx, py * 4 + px) for dy, py in ys for dx, px in xs]
+    return [p for _, p in sorted(both[1:], key=lambda q: -q[0])]
 
 
 def kernel(
@@ -41,7 +40,7 @@
     stream_h, gain1_h, wq_h, wk_h, wv_h, wf_h, fb_h, kc_h, vc_h, gc_h, len_h,
     wo_h, gain2_h, rt_h, rw_h, wg_h, wu_h, wd_h,
     out_ref,
-    stream, gain1, wqkv, wf, fb, kc, vc, gc, lens, wo, gain2, rt, rw, wg, wu, wd,
+    stream, gain1, wqkv, wf, fb, kc, vc, gc, lens, wo, gain2, rt, rw, wgu, wd,
     xn, xin, qs, kvs, qr, kvr, os_, or_, mx, mxr, ss, sr, es, er, fs, fr,
     pick, unpick, spread, comb,
     load_sem, send_sem, recv_sem,
@@ -50,25 +49,15 @@
     seqs, width = stream.shape
     blk = width // ne
     slc = width // nt
+    nz = nt // 2
+    hid = wd.shape[0]
     cache = kc.shape[1]
     hd = kc.shape[2]
     parts = 16 // cap
-    cw = width // parts
+    cw = width // 2 // parts
     g = lax.axis_index("ep")
     t = lax.axis_index("tp")
-
-    barrier = pltpu.get_barrier_semaphore()
-
-    def greet_ep(i, c):
-        pl.semaphore_signal(barrier, inc=1, device_id={"ep": ep_peer(g, i, ne)}, device_id_type=MESH)
-        return c
-
-    def greet_tp(i, c):
-        pl.semaphore_signal(barrier, inc=1, device_id={"tp": tp_peer(t, i, nt)}, device_id_type=MESH)
-        return c
-
-    lax.fori_loop(0, ne - 1, greet_ep, 0)
-    lax.fori_loop(0, nt - 1, greet_tp, 0)
+    z, core = t // 2, lax.rem(t, 2)
 
     loads = [
         (stream_h, stream), (gain1_h, gain1),
@@ -76,10 +65,22 @@
         (wv_h, wqkv.at[:, pl.ds(2 * hd, hd)]),
         (wf_h, wf), (fb_h, fb), (len_h, lens), (rt_h, rt), (rw_h, rw), (gc_h, gc),
         (kc_h, kc), (wo_h, wo), (vc_h, vc), (gain2_h, gain2),
-        (wg_h.at[0], wg), (wu_h.at[0], wu), (wd_h.at[0], wd),
+        (wg_h.at[0], wgu.at[pl.ds(0, hid)]), (wu_h.at[0], wgu.at[pl.ds(hid, hid)]), (wd_h.at[0], wd),
     ]
     copies = [pltpu.make_async_copy(a, b, load_sem.at[i]) for i, (a, b) in enumerate(loads)]
-    for c in copies:
+    copies[0].start()
+    copies[1].start()
+
+    barrier = pltpu.get_barrier_semaphore()
+
+    far_ep = plane(g, ne)
+    far_z = [p for _, p in sorted(ring(z, nz), key=lambda q: -q[0])]
+    far_tp = [2 * p + k for p in far_z for k in range(2)] + [2 * z + 1 - core]
+    for i in range(max(ne, nt) - 1):
+        for axis, peers in (("ep", far_ep), ("tp", far_tp)):
+            if i < len(peers):
+                pl.semaphore_signal(barrier, inc=1, device_id={axis: peers[i]}, device_id_type=MESH)
+    for c in copies[2:]:
         c.start()
     (c_stream, c_gain1, c_q, c_k, c_v, c_wf, c_fb, c_len, c_rt, c_rw, c_gc,
      c_kc, c_wo, c_vc, c_gain2, c_wg, c_wu, c_wd) = copies
@@ -89,28 +90,33 @@
             src_ref=src, dst_ref=dst, send_sem=send_sem.at[phase], recv_sem=recv_sem.at[phase],
             device_id=where, device_id_type=MESH)
 
-    def send_ep(pairs):
-        def body(i, c):
-            peer = ep_peer(g, i, ne)
-            for src, dst, phase in pairs:
-                remote(src.at[peer], dst.at[g], phase, {"ep": peer}).start()
-            return c
-        lax.fori_loop(0, ne - 1, body, 0)
-
-    def send_tp(src, dst, phase, whole=False):
-        def body(i, c):
-            peer = tp_peer(t, i, nt)
-            remote(src if whole else src.at[peer], dst.at[t], phase, {"tp": peer}).start()
-            return c
-        lax.fori_loop(0, nt - 1, body, 0)
-
-    def arrived(buf, phase, axis, n):
-        part = buf.at[pl.ds(0, n - 1)]
-        remote(part, part, phase, {axis: 0}).wait_recv()
-
-    def gone(buf, phase, axis, n):
-        part = buf.at[pl.ds(0, n - 1)]
-        remote(part, part, phase, {axis: 0}).wait_send()
+    def send_ep(src, dst, phase):
+        for peer in far_ep:
+            remote(src.at[peer], dst.at[g], phase, {"ep": peer}).start()
+
+    def send_tp(src, dst, phase):
+        for peer in far_tp:
+            remote(src.at[peer], dst.at[t], phase, {"tp": peer}).start()
+
+    def send_z(src, dst, phase, whole=False):
+        for peer in far_z:
+            remote(src if whole else src.at[peer], dst.at[z], phase, {"tp": 2 * peer + core}).start()
+
+    def send_chips(src, dst, phase, split):
+        for peer in far_ep:
+            for k in range(2):
+                block = src.at[k * ne + peer] if split else src.at[peer]
+                remote(block, dst.at[core * ne + g], phase, {"ep": peer, "tp": 2 * z + k}).start()
+        other = (1 - core) * ne if split else 0
+        remote(src.at[other + g], dst.at[core * ne + g], phase, {"tp": 2 * z + 1 - core}).start()
+
+    def arrived(buf, phase):
+        part = buf.at[pl.ds(0, buf.shape[0] - 1)]
+        remote(part, part, phase, {"ep": 0}).wait_recv()
+
+    def gone(buf, phase):
+        part = buf.at[pl.ds(0, buf.shape[0] - 1)]
+        remote(part, part, phase, {"ep": 0}).wait_send()
 
     c_stream.wait()
     c_gain1.wait()
@@ -120,15 +126,14 @@
     for b in range(ne):
         xn[b] = normed[:, b * blk:(b + 1) * blk]
     pl.semaphore_wait(barrier, ne + nt - 2)
-    send_ep([(xn, xin, 0)])
+    send_ep(xn, xin, 0)
     xin[g] = xn[g]
 
     c_wf.wait()
     c_fb.wait()
     fz = mm(normed, wf[...], NT) + fb[...]
-    heads = fz.shape[1]
-    z = jnp.sum(jnp.where(iota(fz.shape, 1) == t, fz, 0.0), axis=1, keepdims=True)
-    forget = jnp.minimum(z, 0.0) - jnp.log1p(jnp.exp(-jnp.abs(z)))
+    fz = jnp.sum(jnp.where(iota(fz.shape, 1) == t, fz, 0.0), axis=1, keepdims=True)
+    forget = jnp.minimum(fz, 0.0) - jnp.log1p(jnp.exp(-jnp.abs(fz)))
 
     c_len.wait()
     lsq = iota((seqs, seqs), 0) == iota((seqs, seqs), 1)
@@ -184,18 +189,16 @@
     c_q.wait()
     c_k.wait()
     c_v.wait()
-    arrived(xin, 0, "ep", ne)
+    arrived(xin, 0)
     proj = mm(xin[...].reshape(ne * seqs, blk), wqkv[...])
     qs[...] = proj[:, :hd].reshape(ne, seqs, hd)
     kvs[...] = proj[:, hd:].astype(BF16).reshape(ne, seqs, 2 * hd)
-    send_ep([(qs, qr, 1), (kvs, kvr, 2)])
+    send_ep(qs, qr, 1)
+    send_ep(kvs, kvr, 2)
     qr[g] = qs[g]
     kvr[g] = kvs[g]
-    arrived(qr, 1, "ep", ne)
-    arrived(kvr, 2, "ep", ne)
+    arrived(qr, 1)
     query = jnp.sum(qr[...], axis=0).astype(BF16)
-    kv = jnp.sum(kvr[...].astype(F32), axis=0).astype(BF16)
-    key_new, value_new = kv[:, :hd], kv[:, hd:]
 
     scale = hd ** (-0.5)
     c_kc.wait()
@@ -204,6 +207,9 @@
         scores = jnp.where(row == s, mm(query, kc[s], NT), scores)
     scores = scores * scale + forget + last_gate - gates
     scores = jnp.where(live, scores, -1e30)
+    arrived(kvr, 2)
+    kv = jnp.sum(kvr[...].astype(F32), axis=0).astype(BF16)
+    key_new, value_new = kv[:, :hd], kv[:, hd:]
     own = jnp.sum(query.astype(F32) * key_new.astype(F32), axis=1, keepdims=True) * scale
     top = jnp.maximum(jnp.max(scores, axis=1, keepdims=True), own)
     past = jnp.exp(scores - top)
@@ -225,52 +231,59 @@
     send_tp(os_, or_, 3)
     or_[t] = os_[t]
     own_stream = stream[:, pl.ds(pl.multiple_of(t * slc, slc), slc)].astype(F32)
-    arrived(or_, 3, "tp", nt)
+    arrived(or_, 3)
     mixed = (own_stream + jnp.sum(or_[...].astype(F32), axis=0)).astype(BF16)
     mx[...] = mixed
-    send_tp(mx, mxr, 4, whole=True)
-    mxr[t] = mixed
-    arrived(mxr, 4, "tp", nt)
-
-    per = nt // parts
+    send_z(mx, mxr, 4, whole=True)
+    mxr[z] = mixed
+    arrived(mxr, 4)
+
+    per = nz // parts
     stacked = jnp.concatenate(
         [jnp.concatenate([mxr[j * per + u] for u in range(per)], axis=1) for j in range(parts)], axis=0)
     ss[...] = mm(pick[...], stacked).astype(BF16).reshape(ne, 16, cw)
-    send_ep([(ss, sr, 5)])
-    sr[g] = ss[g]
+    send_chips(ss, sr, 5, False)
+    sr[core * ne + g] = ss[g]
     c_gain2.wait()
     c_wg.wait()
     c_wu.wait()
-    arrived(sr, 5, "ep", ne)
-    rows_in = mm(unpick[...], sr[...].reshape(lanes, cw))
-    xs = jnp.concatenate([rows_in[j * rows:(j + 1) * rows] for j in range(parts)], axis=1)
+    arrived(sr, 5)
+    halves = [mm(unpick[...], sr[pl.ds(k * ne, ne)].reshape(lanes, cw)) for k in range(2)]
+    xs = []
+    for u in range(nt):
+        j, v = u // 2 // per, u // 2 % per
+        xs.append(halves[u % 2][j * rows:(j + 1) * rows, v * slc:(v + 1) * slc])
+    xs = jnp.concatenate(xs, axis=1)
     rs2 = lax.rsqrt(jnp.mean(xs * xs, axis=-1, keepdims=True) + 1e-06)
     xs = (xs * rs2 * gain2[...]).astype(BF16)
-    gate = mm(xs, wg[...], NT)
-    up = mm(xs, wu[...], NT)
+    gate = mm(xs, wgu[pl.ds(0, hid)], NT)
+    up = mm(xs, wgu[pl.ds(hid, hid)], NT)
     hidden = (gate / (1.0 + jnp.exp(-gate)) * up).astype(BF16)
     c_wd.wait()
     part = mm(hidden, wd[...]).astype(BF16)
-    part = jnp.concatenate([part[:, j * cw:(j + 1) * cw] for j in range(parts)], axis=0)
-    es[...] = mm(spread[...], part).astype(BF16).reshape(ne, 16, cw)
-    send_ep([(es, er, 6)])
-    er[g] = es[g]
-    arrived(er, 6, "ep", ne)
-
-    both = mm(comb[...], er[...].reshape(lanes, cw))
+    piled = []
+    for k in range(2):
+        piled.append(jnp.concatenate([
+            jnp.concatenate([part[:, (2 * (j * per + v) + k) * slc:][:, :slc] for v in range(per)], axis=1)
+            for j in range(parts)], axis=0))
+    for k in range(2):
+        es[pl.ds(k * ne, ne)] = mm(spread[...], piled[k]).astype(BF16).reshape(ne, 16, cw)
+    send_chips(es, er, 6, True)
+    er[core * ne + g] = es[core * ne + g]
+    arrived(er, 6)
+    both = (mm(comb[...], er[pl.ds(0, ne)].reshape(lanes, cw))
+            + mm(comb[...], er[pl.ds(ne, ne)].reshape(lanes, cw)))
     for j in range(parts):
         piece = (both[2 * j * seqs:(2 * j + 1) * seqs] + both[(2 * j + 1) * seqs:(2 * j + 2) * seqs]).astype(BF16)
         for u in range(per):
             fs[j * per + u] = piece[:, u * slc:(u + 1) * slc]
-    send_tp(fs, fr, 7)
-    fr[t] = fs[t]
-    arrived(fr, 7, "tp", nt)
+    send_z(fs, fr, 7)
+    fr[z] = fs[z]
+    arrived(fr, 7)
     out_ref[...] = (mixed.astype(F32) + jnp.sum(fr[...].astype(F32), axis=0)).astype(BF16)
 
-    for buf, phase, axis, n in (
-        (xin, 0, "ep", ne), (qr, 1, "ep", ne), (kvr, 2, "ep", ne), (or_, 3, "tp", nt),
-        (mxr, 4, "tp", nt), (sr, 5, "ep", ne), (er, 6, "ep", ne), (fr, 7, "tp", nt)):
-        gone(buf, phase, axis, n)
+    for phase, buf in enumerate((xin, qr, kvr, or_, mxr, sr, er, fr)):
+        gone(buf, phase)
 
 
 def shards(
@@ -284,7 +297,7 @@
     cap = 2 * seqs * tops // ne
     blk, slc, hid = width // ne, width // nt, w_expert_gate.shape[2]
     parts = 16 // cap
-    cw = width // parts
+    cw = width // 2 // parts
     args = (
         stream, norm_gain_attn.reshape(1, -1), w_query, w_key, w_value, w_forget.T,
         forget_bias.reshape(1, -1), key_cache, value_cache, gate_cache, lengths.reshape(1, -1),
@@ -298,15 +311,15 @@
         V(key_cache.shape, BF16), V(value_cache.shape, BF16), V(gate_cache.shape, F32),
         V((1, seqs), jnp.int32), V(w_output.shape, BF16), V((1, width), F32),
         V(routes.shape[::-1], jnp.int32), V(routes.shape[::-1], F32),
-        V((hid, width), BF16), V((hid, width), BF16), V((hid, width), BF16),
+        V((2 * hid, width), BF16), V((hid, width), BF16),
         V((ne, seqs, blk), BF16), V((ne, seqs, blk), BF16),
         V((ne, seqs, hd), F32), V((ne, seqs, 2 * hd), BF16),
         V((ne, seqs, hd), F32), V((ne, seqs, 2 * hd), BF16),
         V((nt, seqs, slc), BF16), V((nt, seqs, slc), BF16),
-        V((seqs, slc), BF16), V((nt, seqs, slc), BF16),
-        V((ne, 16, cw), BF16), V((ne, 16, cw), BF16),
-        V((ne, 16, cw), BF16), V((ne, 16, cw), BF16),
-        V((nt, seqs, slc), BF16), V((nt, seqs, slc), BF16),
+        V((seqs, slc), BF16), V((nt // 2, seqs, slc), BF16),
+        V((ne, 16, cw), BF16), V((2 * ne, 16, cw), BF16),
+        V((2 * ne, 16, cw), BF16), V((2 * ne, 16, cw), BF16),
+        V((nt // 2, seqs, slc), BF16), V((nt // 2, seqs, slc), BF16),
         V((ne * 16, parts * seqs), BF16), V((parts * ne * cap, ne * 16), BF16),
         V((ne * 16, parts * ne * cap), BF16), V((2 * parts * seqs, ne * 16), BF16),
         pltpu.SemaphoreType.DMA((18,)), pltpu.SemaphoreType.DMA((8,)), pltpu.SemaphoreType.DMA((8,)),
@@ -314,11 +327,11 @@
     return pl.pallas_call(
         functools.partial(kernel, (ne, nt, cap)),
         out_shape=jax.ShapeDtypeStruct((seqs, slc), BF16),
-        in_specs=[pl.BlockSpec(memory_space=pl.ANY)] * len(args),
+        in_specs=[pl.BlockSpec(memory_space=pltpu.HBM)] * len(args),
         out_specs=pl.BlockSpec(memory_space=pltpu.VMEM),
         scratch_shapes=scratch,
         compiler_params=pltpu.CompilerParams(
-            collective_id=0, has_side_effects=True, vmem_limit_bytes=48 * 1024 * 1024),
+            collective_id=0, has_side_effects=True, vmem_limit_bytes=67043328),
         name="layer",
     )(*args)
 

time: 66.2 us -> 50.6 us (0.76)
  local copies, waits for them, and re-layouts: 14.6 us -> 1.28 us
  Pallas kernels: 50.9 us -> 49.2 us
    unnamed x33 -> x1, local copies, waits for them, and re-layouts: 14.6 us -> 1.28 us
    pallas_call x1, Pallas kernels: 50.9 us -> 49.2 us  [shards(): pl.pallas_call(functools.partial(kernel, (ne, nt, cap)), out_shape=jax.Sh...]
where the time goes in v2:
time: 50.6 us; the launch traced here: 50.5 us
  Pallas kernels  49.2 us (97%)
  local copies, waits for them, and re-layouts  1.28 us (3%)
    pallas_call x1, Pallas kernels, shards(): pl.pallas_call(functools.partial(kernel, (ne, nt, cap)), out_shape=jax.Sh...  49.2 us
    unnamed x1, local copies, waits for them, and re-layouts  1.28 us

profile of v2, /device:TPU:1, one launch (start us, length us, event | category | flops | bytes accessed | tf_op | source)
XLA Modules:
  0.0 50.5 jit_solution(12481456502145140465)
XLA Ops:
  0.0 49.2 %layer.1 = bf16[16,128]{1,0:T(8,128)(2,1)} custom-call(bf16[16,2048]{1,0:T(8,128)(2,1)} %stream_h.1, f32[1,2048]{1,0:T(1,128)} %bitcast.12, bf16[128,128]{1,0:T(8,128)(2,1)} %wq_h.1, bf16[128,128]{1,0:T(8,128)(2,1)} %wk_h.1, bf16[128,128]{1,0:T(8,128)(2,1)} %wv_h.1, bf16[16,2048]{1,0:T(8,128)(2,1)} %bitcast.11, f32[1,16]{1,0:T(1,128)} %bitcast.16, ...), custom_call_target="tpu_custom_call" | custom-call | tf_op jit(solution)/shard_map/layer/pallas_call | solution.py:327
  49.2 1.3 %copy.20 = bf16[16,128]{1,0:T(8,128)(2,1)} copy(bf16[16,128]{1,0:T(8,128)(2,1)} %layer.1) | data formatting | bytes 8192
